TPU v7x, 32 devices: a whole 2x2x4 slice. The times are simulated.
32 devices in a mesh: tp: 8 (over z, y), dp: 4 (over x, core).
Axes of the slice: x: 2, y: 2, z: 4, core: 2. Of those that a mesh axis runs over, the one named last changes fastest.
Arguments:
- tokens: bfloat16 [64, 4096], P('tp', 'dp'), may hold values from -30 to 30
- lengths: int32 [64], P('dp'), may hold values from 1 to 2048, 16384 in all
- states: float32 [2, 64, 2048, 128], P(None, 'dp', 'tp'), may hold values from -0.8 to 0.8
- norm_gain: bfloat16 [2, 4096], P(None, 'dp'), may hold values from 0.099609375 to 1.8984375
- w_query: bfloat16 [2, 4096, 2048], P(None, 'dp', 'tp'), may hold values from -0.09375 to 0.09375
- w_key: bfloat16 [2, 4096, 2048], P(None, 'dp', 'tp'), may hold values from -0.09375 to 0.09375
- w_value: bfloat16 [2, 4096, 2048], P(None, 'dp', 'tp'), may hold values from -0.09375 to 0.09375
- w_gate: bfloat16 [2, 4096, 2048], P(None, 'dp', 'tp'), may hold values from -0.09375 to 0.09375
- head_gain: bfloat16 [2, 2048], P(None, 'tp'), may hold values from 0.099609375 to 1.8984375
- w_out: bfloat16 [2, 2048, 4096], P(None, 'tp', 'dp'), may hold values from -0.125 to 0.125
Outputs:
- hidden_out: bfloat16 [64, 4096], P('tp', 'dp')
- new_states: float32 [2, 64, 2048, 128], P(None, 'dp', 'tp')
All inputs are finite; a program needn't handle non-finite values. No bound on the sum of `lengths` on one device may be relied on, other than what follows from the above.
Results may differ from a plain program's by a relative error of at most 0.012.
Values may be sent and summed in bfloat16 or wider, within the bound.
No kernel may reach another device: no remote copies, remote signals or barrier semaphores. Data moves between devices by JAX's collectives and lax.ppermute only.
A program may use at most 64 MiB of HBM per device.

v0:
```python
import jax
import jax.numpy as jnp
from jax import lax
from jax.sharding import PartitionSpec as P

D = 4096
HEADS = 16
DK = 128
LAYERS = 2


norm_eps = 1e-06
group_eps = 1e-05
rotary_base = 10000.0


def partner_2(value, axis, apart):
    mask = 2**apart
    pairs = [(source, source ^ mask) for source in range(lax.axis_size(axis))]
    return lax.ppermute(value, axis, pairs)


def rotate(values, positions):
    half_size = values.shape[-1] // 2
    inverse = rotary_base ** (-jnp.arange(half_size, dtype=jnp.float32) / half_size)
    angles = positions.astype(jnp.float32)[:, None] * inverse[None, :]
    cosine = jnp.cos(angles)[:, None, :]
    sine_v = jnp.sin(angles)[:, None, :]
    first_part = values[..., :half_size]
    second = values[..., half_size:]
    return jnp.concatenate(
        [first_part * cosine - second * sine_v, first_part * sine_v + second * cosine], axis=-1
    )


def decays(head_ids):
    return 1.0 - jnp.exp2(-1.0 - 9.0 * head_ids.astype(jnp.float32) / (HEADS - 1))


def body(tokens, lengths, states, norm_gain, w_query, w_key, w_value, w_gate, head_gain, w_out):
    tp_index = lax.axis_index("tp")
    dp_index = lax.axis_index("dp")
    tp_count = lax.axis_size("tp")
    columns = w_query.shape[2]
    pieces = max(DK // columns, 1)
    levels = pieces.bit_length() - 1
    local_heads = max(columns // DK, 1)
    value_cols = columns // local_heads
    head_ids = tp_index * columns // DK + jnp.arange(local_heads, dtype=jnp.int32)
    gammas = decays(head_ids)
    hidden_x = tokens
    outputs = []
    for layer_id in range(LAYERS):
        prior_state = states[layer_id]
        row_total = prior_state.shape[0]
        local_rows = hidden_x.shape[0]
        x_float = hidden_x.astype(jnp.float32)
        feature_gain = norm_gain[layer_id].astype(jnp.float32)
        weights = jnp.concatenate(
            [w_query[layer_id], w_key[layer_id], w_value[layer_id], w_gate[layer_id]], axis=1
        )
        gathered = lax.all_gather(hidden_x, "tp", axis=0, tiled=True)
        gathered_f = gathered.astype(jnp.float32)
        normed = (gathered_f * feature_gain).astype(jnp.bfloat16)
        partial_value = jnp.dot(normed, weights, preferred_element_type=jnp.float32)
        squares_full = jnp.zeros((local_rows * tp_count,), jnp.float32)
        squares_full = lax.dynamic_update_slice_in_dim(
            squares_full, jnp.sum(x_float * x_float, axis=1), tp_index * local_rows, 0
        )
        all_squares = lax.psum(squares_full, ("tp", "dp"))
        summed = lax.psum_scatter(partial_value, "dp", scatter_dimension=0, tiled=True)
        own_squares = lax.dynamic_slice_in_dim(all_squares, dp_index * row_total, row_total, 0)
        row_scale = lax.rsqrt(own_squares / D + norm_eps)
        projected = (summed * row_scale[:, None]).astype(jnp.bfloat16)
        query_rows = projected[:, :columns]
        key_rows = projected[:, columns : 2 * columns]
        value_rows = projected[:, 2 * columns : 3 * columns]
        gate_rows = projected[:, 3 * columns :]
        stacked = jnp.stack([query_rows, key_rows])
        for join_level_id in range(levels):
            partner = partner_2(stacked, "tp", join_level_id)
            upper_bit = tp_index // 2**join_level_id % 2
            stacked = jnp.where(
                upper_bit == 1,
                jnp.concatenate([partner, stacked], axis=-1),
                jnp.concatenate([stacked, partner], axis=-1),
            )
        query_f = rotate(
            stacked[0].astype(jnp.float32).reshape(row_total, local_heads, DK), lengths
        )
        key_f = rotate(
            stacked[1].astype(jnp.float32).reshape(row_total, local_heads, DK), lengths
        ) * DK ** (-0.5)
        values_f = value_rows.astype(jnp.float32).reshape(row_total, local_heads, value_cols)
        state_view = prior_state.reshape(row_total, local_heads, value_cols, DK)
        updated = gammas[None, :, None, None] * state_view + jnp.einsum(
            "shd,shv->shvd", key_f, values_f
        )
        readout = jnp.einsum("shd,shvd->shv", query_f, updated)
        head_stats = jnp.stack([jnp.sum(readout, axis=-1), jnp.sum(readout * readout, axis=-1)])
        for level_id in range(levels):
            head_stats = head_stats + partner_2(head_stats, "tp", level_id)
        mean_v = head_stats[0][..., None] / DK
        square = head_stats[1][..., None] / DK
        grouped = ((readout - mean_v) * lax.rsqrt(square - mean_v * mean_v + group_eps)).reshape(
            row_total, columns
        )
        grouped = grouped * head_gain[layer_id].astype(jnp.float32)
        gated_rows = (jax.nn.silu(gate_rows.astype(jnp.float32)) * grouped).astype(jnp.bfloat16)
        out_weight = w_out[layer_id]
        whole_weight = lax.all_gather(out_weight, "tp", axis=0, tiled=True)
        every_row = lax.all_gather(gated_rows, "dp", axis=0, tiled=True)
        owned_rows = lax.all_to_all(every_row, "tp", split_axis=0, concat_axis=1, tiled=True)
        branch = jnp.dot(owned_rows, whole_weight, preferred_element_type=jnp.float32)
        hidden_x, updated = (
            (x_float + branch).astype(jnp.bfloat16),
            updated.reshape(row_total, columns, DK),
        )
        outputs.append(updated)
    return (hidden_x, jnp.stack(outputs))


def solution(mesh):
    placed = (
        P("tp", "dp"),
        P("dp"),
        P(None, "dp", "tp", None),
        P(None, "dp"),
        P(None, "dp", "tp"),
        P(None, "dp", "tp"),
        P(None, "dp", "tp"),
        P(None, "dp", "tp"),
        P(None, "tp"),
        P(None, "tp", "dp"),
    )
    return jax.shard_map(
        body,
        mesh=mesh,
        in_specs=placed,
        out_specs=(P("tp", "dp"), P(None, "dp", "tp", None)),
        check_vma=False,
    )
```

profile of v0, /device:TPU:0, one launch (start us, length us, event | category | flops | bytes accessed | tf_op | source)
XLA Modules:
  0.0 245.5 jit_solution(17588440073124180432)
XLA Ops:
  8.0 32.5 %all_gather.18 = bf16[64,1024]{1,0:T(8,128)(2,1)S(1)} all-gather(bf16[8,1024]{1,0:T(8,128)(2,1)} %param.10), channel_id=1, replica_groups=mesh['tp'=8,'dp'=4] {'tp'}, dimensions={0}, use_global_device_ids=true | all-gather | bytes 147456 | tf_op jit(solution)/shard_map/all_gather | solution.py:62
  40.6 0.8 slice_convert_fusion.6
  41.4 1.8 slice_bitcast_fusion.4
  43.2 0.3 copy-done.3
  43.5 1.1 slice_bitcast_fusion.6
  44.6 1.2 fusion.4
  45.9 1.1 fusion.51
  47.3 0.2 dynamic_update_slice.6
  47.5 41.5 %psum.14 = f32[64]{0:T(128)S(1)} all-reduce(f32[64]{0:T(128)S(1)} %dynamic_update_slice.6), channel_id=1, replica_groups=mesh['tp'=8,'dp'=4] {'tp','dp'}, use_global_device_ids=true, to_apply=%region_2.3 | all-reduce | flops 64 | bytes 512 | tf_op jit(solution)/shard_map/psum | solution.py:70
  89.3 4.7 %fusion.50 = (f32[1,16,256,128]{3,2,1,0:T(8,128)}, f32[1,16,256,128]{3,2,1,0:T(8,128)}) fusion(f32[2,16,256,128]{3,2,1,0:T(8,128)} %param.12), kind=kLoop, calls=%fused_computation.101 | loop fusion | bytes 8388608 | tf_op jit(solution)/shard_map/slice | solution.py:54
  94.0 0.9 multiply_convert_fusion.5
  95.3 2.0 multiply_add_fusion.1
  97.2 0.6 fusion.52
  97.9 0.1 fusion.49
  98.1 5.5 %all_gather.19 = bf16[64,256]{1,0:T(8,128)(2,1)S(1)} all-gather(bf16[16,256]{1,0:T(8,128)(2,1)S(1)} %fusion.45), channel_id=1, replica_groups=mesh['tp'=8,'dp'=4] {'dp'}, dimensions={0}, use_global_device_ids=true | all-gather | bytes 40960 | tf_op jit(solution)/shard_map/all_gather | solution.py:112
  103.6 13.0 %all_to_all.38 = bf16[8,8,256]{2,1,0:T(8,128)(2,1)S(1)} all-to-all(bf16[8,8,256]{2,1,0:T(8,128)(2,1)S(1)} %bitcast.88), channel_id=1, replica_groups=mesh['tp'=8,'dp'=4] {'tp'}, dimensions={0} | all-to-all | bytes 65536 | tf_op jit(solution)/shard_map/all_to_all | solution.py:113
  116.7 8.1 %all-gather.5.cloned.1.call-done = bf16[1,2048,1024]{2,1,0:T(8,128)(2,1)} async-done(((bf16[1,256,1024]{2,1,0:T(8,128)(2,1)}), bf16[1,2048,1024]{2,1,0:T(8,128)(2,1)}) %all-gather.5.cloned.1.call-update) | async-done | bytes 4194320 | tf_op jit(solution)/shard_map/all_gather | solution.py:111
  124.8 3.0 %fusion.35 = (f32[8]{0:T(128)S(1)}, bf16[8,1024]{1,0:T(8,128)(2,1)S(1)}) fusion(bf16[8,2048]{1,0:T(8,128)(2,1)S(1)} %bitcast.87, bf16[1,2048,1024]{2,1,0:T(8,128)(2,1)} %all-gather.5.cloned.1.call-done, bf16[8,1024]{1,0:T(8,128)(2,1)S(1)} %copy-done.6), kind=kOutput, calls=%fused_computation.44 | convolution fusion | flops 33603576 | bytes 4259872 | tf_op jit(solution)/shard_map/dot_general | solution.py:114
  127.8 30.6 %all_gather.21 = bf16[64,1024]{1,0:T(8,128)(2,1)S(1)} all-gather(bf16[8,1024]{1,0:T(8,128)(2,1)S(1)} %get-tuple-element.47), channel_id=1, replica_groups=mesh['tp'=8,'dp'=4] {'tp'}, dimensions={0}, use_global_device_ids=true | all-gather | bytes 147456 | tf_op jit(solution)/shard_map/all_gather | solution.py:62
  158.4 1.2 fusion.12
  159.7 0.5 all-gather.7.cloned.1.call-update
  160.2 0.2 dynamic_update_slice.7
  160.5 38.9 %psum.15 = f32[64]{0:T(128)S(1)} all-reduce(f32[64]{0:T(128)S(1)} %dynamic_update_slice.7), channel_id=1, replica_groups=mesh['tp'=8,'dp'=4] {'tp','dp'}, use_global_device_ids=true, to_apply=%region_7.8 | all-reduce | flops 64 | bytes 512 | tf_op jit(solution)/shard_map/psum | solution.py:70
  199.5 0.9 multiply_convert_fusion.4
  200.7 2.0 multiply_add_fusion
  202.7 1.3 copy-done
  204.0 0.6 fusion.53
  204.9 5.9 %all_gather.22 = bf16[64,256]{1,0:T(8,128)(2,1)} all-gather(bf16[16,256]{1,0:T(8,128)(2,1)S(1)} %fusion.44), channel_id=1, replica_groups=mesh['tp'=8,'dp'=4] {'dp'}, dimensions={0}, use_global_device_ids=true | all-gather | bytes 40960 | tf_op jit(solution)/shard_map/all_gather | solution.py:112
  210.8 6.1 %all-to-all-start.1 = ((bf16[8,8,256]{2,1,0:T(8,128)(2,1)}), bf16[8,8,256]{2,1,0:T(8,128)(2,1)S(1)}, u32[]{:S(2)}, u32[]{:S(2)}) async-start(bf16[8,8,256]{2,1,0:T(8,128)(2,1)} %bitcast.26), calls=%async_computation.3 | async-start | bytes 65536 | tf_op jit(solution)/shard_map/all_to_all | solution.py:113
  216.9 4.0 %pad_maximum_fusion = f32[2,16,256,128]{3,2,1,0:T(8,128)} fusion(f32[1,16,256,128]{3,2,1,0:T(8,128)} %bitcast.79, f32[1,16,256,128]{3,2,1,0:T(8,128)S(1)} %bitcast.78), kind=kLoop, calls=%fused_computation | loop fusion | flops 1048576 | bytes 8388608 | tf_op jit(solution)/shard_map/stack | solution.py:120
  220.9 13.7 %all-gather.7.cloned.1.call-done = bf16[1,2048,1024]{2,1,0:T(8,128)(2,1)} async-done(((bf16[1,256,1024]{2,1,0:T(8,128)(2,1)}), bf16[1,2048,1024]{2,1,0:T(8,128)(2,1)}) %all-gather.7.cloned.1.call-update) | async-done | bytes 4194320 | tf_op jit(solution)/shard_map/all_gather | solution.py:111
  234.6 3.5 %fusion.26 = bf16[8,1024]{1,0:T(8,128)(2,1)} fusion(bf16[8,2048]{1,0:T(8,128)(2,1)S(1)} %bitcast.86, bf16[1,2048,1024]{2,1,0:T(8,128)(2,1)} %all-gather.7.cloned.1.call-done, bf16[8,1024]{1,0:T(8,128)(2,1)S(1)} %get-tuple-element.47), kind=kOutput, calls=%fused_computation.25 | convolution fusion | flops 33579008 | bytes 4259840 | tf_op jit(solution)/shard_map/dot_general | solution.py:114
  (57 shorter events, 1.7 us)
Async XLA Ops:
  8.0 86.0 %reduce-scatter.3.cloned.1.call-start = ((), (), s32[]{:S(2)}) async-start(), calls=%async_computation.4 | async-start | bytes 327680 | tf_op jit(solution)/shard_map/reduce_scatter | solution.py:71
  41.4 1.9 copy-start.2
  41.4 2.2 copy-start.3
  44.6 1.3 copy-start.1
  45.8 1.3 copy-start.8
  45.8 1.3 copy-start.6
  45.8 43.3 %copy-start.7 = (bf16[2,256]{1,0:T(2,128)(2,1)S(1)}, bf16[2,256]{1,0:T(2,128)(2,1)}, u32[]{:S(2)}) copy-start(bf16[2,256]{1,0:T(2,128)(2,1)} %param.18) | copy-start | bytes 3076
  45.9 78.9 %all-gather.5.cloned.1.call-start = ((), (), s32[]{:S(2)}) async-start(), calls=%async_computation.6 | async-start | bytes 4718592 | tf_op jit(solution)/shard_map/all_gather | solution.py:111
  47.0 152.4 %reduce-scatter.5.cloned.1.call-start = ((), (), s32[]{:S(2)}) async-start(), calls=%async_computation.5 | async-start | bytes 327680 | tf_op jit(solution)/shard_map/reduce_scatter | solution.py:71
  124.8 33.6 %copy-start.4 = (bf16[1024,256]{1,0:T(8,128)(2,1)S(1)}, bf16[1024,256]{1,0:T(8,128)(2,1)}, u32[]{:S(2)}) copy-start(bf16[1024,256]{1,0:T(8,128)(2,1)} %get-tuple-element.13) | copy-start | bytes 1572868
  124.8 33.6 %copy-start.5 = (bf16[1024,256]{1,0:T(8,128)(2,1)S(1)}, bf16[1024,256]{1,0:T(8,128)(2,1)}, u32[]{:S(2)}) copy-start(bf16[1024,256]{1,0:T(8,128)(2,1)} %get-tuple-element.50) | copy-start | bytes 1572868
  159.6 75.0 %all-gather.7.cloned.1.call-start = ((), (), s32[]{:S(2)}) async-start(), calls=%async_computation.7 | async-start | bytes 4718592 | tf_op jit(solution)/shard_map/all_gather | solution.py:111
  202.7 1.3 copy-start
  210.8 23.8 %all-to-all-start.1 = ((bf16[8,8,256]{2,1,0:T(8,128)(2,1)}), bf16[8,8,256]{2,1,0:T(8,128)(2,1)S(1)}, u32[]{:S(2)}, u32[]{:S(2)}) async-start(bf16[8,8,256]{2,1,0:T(8,128)(2,1)} %bitcast.26), calls=%async_computation.3 | async-start | bytes 65536 | tf_op jit(solution)/shard_map/all_to_all | solution.py:113
Sparse Core Ops, SparseCore 0:
  46.0 20.9 reduce-scatter.2
  159.7 17.8 reduce-scatter.4
Sparse Core Ops, SparseCore 1:
  48.5 76.2 all-gather.4
  162.2 72.3 all-gather.6
where the time goes:
time: 246 us; the launch traced here: 245 us
  blocking collectives  168 us (68%)
  waiting for transfers between devices  22.4 us (9%)
  between operations  15.7 us (6%)
  other arithmetic  12 us (5%)
  local copies, waits for them, and re-layouts  11 us (4%)
  matrix products  10.1 us (4%)
  starting transfers between devices  6.26 us (3%)
    psum x2, blocking collectives, body(): all_squares = lax.psum(squares_full, ('tp', 'dp'))  80.4 us
    all_gather x2, blocking collectives, body(): gathered = lax.all_gather(hidden_x, 'tp', axis=0, tiled=True)  63.1 us
    all_gather x2, waiting for transfers between devices, body(): whole_weight = lax.all_gather(out_weight, 'tp', axis=0, tiled=True)  21.9 us
    all_to_all x1, blocking collectives, body(): lax.all_to_all(every_row, 'tp', split_axis=0, concat_axis=1, tiled=True)  13 us
    all_gather x2, blocking collectives, body(): every_row = lax.all_gather(gated_rows, 'dp', axis=0, tiled=True)  11.4 us
    dot_general x2, matrix products, body(): jnp.dot(owned_rows, whole_weight, preferred_element_type=jnp.float32)  6.49 us
    all_to_all x1, starting transfers between devices, body(): lax.all_to_all(every_row, 'tp', split_axis=0, concat_axis=1, tiled=True)  6.09 us
  transfers between devices with their start and end apart: 5, of which 2 were waited for; matrix products, arithmetic and copies ran while one was open for 8% of the time, Pallas kernels for 0%

commit v1 on v0

--- a/solution.py
+++ b/solution.py
@@ -37,10 +37,20 @@
     return 1.0 - jnp.exp2(-1.0 - 9.0 * head_ids.astype(jnp.float32) / (HEADS - 1))
 
 
+def gather_rows(value, axis):
+    return lax.all_gather(value, axis, axis=0, tiled=True)
+
+
+def sum_rows(partial_value, axis):
+    count = lax.axis_size(axis)
+    rows = partial_value.shape[0] // count
+    split = partial_value.reshape(count, rows, partial_value.shape[1])
+    swapped = lax.all_to_all(split, axis, split_axis=0, concat_axis=0, tiled=True)
+    return jnp.sum(swapped.astype(jnp.float32), axis=0)
+
+
 def body(tokens, lengths, states, norm_gain, w_query, w_key, w_value, w_gate, head_gain, w_out):
     tp_index = lax.axis_index("tp")
-    dp_index = lax.axis_index("dp")
-    tp_count = lax.axis_size("tp")
     columns = w_query.shape[2]
     pieces = max(DK // columns, 1)
     levels = pieces.bit_length() - 1
@@ -53,25 +63,19 @@
     for layer_id in range(LAYERS):
         prior_state = states[layer_id]
         row_total = prior_state.shape[0]
-        local_rows = hidden_x.shape[0]
-        x_float = hidden_x.astype(jnp.float32)
-        feature_gain = norm_gain[layer_id].astype(jnp.float32)
-        weights = jnp.concatenate(
-            [w_query[layer_id], w_key[layer_id], w_value[layer_id], w_gate[layer_id]], axis=1
-        )
-        gathered = lax.all_gather(hidden_x, "tp", axis=0, tiled=True)
-        gathered_f = gathered.astype(jnp.float32)
-        normed = (gathered_f * feature_gain).astype(jnp.bfloat16)
-        partial_value = jnp.dot(normed, weights, preferred_element_type=jnp.float32)
-        squares_full = jnp.zeros((local_rows * tp_count,), jnp.float32)
-        squares_full = lax.dynamic_update_slice_in_dim(
-            squares_full, jnp.sum(x_float * x_float, axis=1), tp_index * local_rows, 0
-        )
-        all_squares = lax.psum(squares_full, ("tp", "dp"))
-        summed = lax.psum_scatter(partial_value, "dp", scatter_dimension=0, tiled=True)
-        own_squares = lax.dynamic_slice_in_dim(all_squares, dp_index * row_total, row_total, 0)
+        gathered_f = gather_rows(hidden_x, "tp").astype(jnp.float32)
+        normed = (gathered_f * norm_gain[layer_id].astype(jnp.float32)).astype(jnp.bfloat16)
+        squares = jnp.sum(gathered_f * gathered_f, axis=1, keepdims=True)
+        high = squares.astype(jnp.bfloat16)
+        low = (squares - high.astype(jnp.float32)).astype(jnp.bfloat16)
+        blocks = [
+            jnp.dot(normed, w[layer_id], preferred_element_type=jnp.float32).astype(jnp.bfloat16)
+            for w in (w_query, w_key, w_value, w_gate)
+        ]
+        summed = sum_rows(jnp.concatenate(blocks + [high, low], axis=1), "dp")
+        own_squares = summed[:, 4 * columns] + summed[:, 4 * columns + 1]
         row_scale = lax.rsqrt(own_squares / D + norm_eps)
-        projected = (summed * row_scale[:, None]).astype(jnp.bfloat16)
+        projected = (summed[:, : 4 * columns] * row_scale[:, None]).astype(jnp.bfloat16)
         query_rows = projected[:, :columns]
         key_rows = projected[:, columns : 2 * columns]
         value_rows = projected[:, 2 * columns : 3 * columns]
@@ -107,16 +111,11 @@
         )
         grouped = grouped * head_gain[layer_id].astype(jnp.float32)
         gated_rows = (jax.nn.silu(gate_rows.astype(jnp.float32)) * grouped).astype(jnp.bfloat16)
-        out_weight = w_out[layer_id]
-        whole_weight = lax.all_gather(out_weight, "tp", axis=0, tiled=True)
-        every_row = lax.all_gather(gated_rows, "dp", axis=0, tiled=True)
-        owned_rows = lax.all_to_all(every_row, "tp", split_axis=0, concat_axis=1, tiled=True)
-        branch = jnp.dot(owned_rows, whole_weight, preferred_element_type=jnp.float32)
-        hidden_x, updated = (
-            (x_float + branch).astype(jnp.bfloat16),
-            updated.reshape(row_total, columns, DK),
-        )
-        outputs.append(updated)
+        every_row = gather_rows(gated_rows, "dp")
+        branch_parts = jnp.dot(every_row, w_out[layer_id], preferred_element_type=jnp.float32)
+        branch = sum_rows(branch_parts.astype(jnp.bfloat16), "tp")
+        hidden_x = (hidden_x.astype(jnp.float32) + branch).astype(jnp.bfloat16)
+        outputs.append(updated.reshape(row_total, columns, DK))
     return (hidden_x, jnp.stack(outputs))
 
 

time: 246 us -> 133 us (0.54)
  blocking collectives: 168 us -> 94.2 us
  waiting for transfers between devices: 22.4 us -> 3.74 us
  between operations: 15.7 us -> 1.09 us
  local copies, waits for them, and re-layouts: 11 us -> 8.03 us
  matrix products: 10.1 us -> 7.19 us
    psum x2 -> x0, blocking collectives: 80.4 us -> none  [body(): all_squares = lax.psum(squares_full, ('tp', 'dp'))]
    all_gather x2 -> x0, waiting for transfers between devices: 21.9 us -> none  [body(): whole_weight = lax.all_gather(out_weight, 'tp', axis=0, tiled=True)]
    all_to_all x1 -> x2, blocking collectives: 13 us -> 20.6 us  [sum_rows(): lax.all_to_all(split, axis, split_axis=0, concat_axis=0, tiled=True)]
    all_to_all x1 -> x2, waiting for transfers between devices: 0.01 us -> 3.74 us  [sum_rows(): lax.all_to_all(split, axis, split_axis=0, concat_axis=0, tiled=True)]
    dot_general x4 -> x10, matrix products: 8.85 us -> 5.92 us  [the longest x8 4.85 us: body(): jnp.dot(normed, w[layer_id], preferred_element_type=jnp.float32)]
    squeeze x2 -> x0, local copies, waits for them, and re-layouts: 2.91 us -> none  [the longest x1 1.8 us: body(): w_gate[layer_id]]
    all_to_all x1 -> x2, starting transfers between devices: 6.09 us -> 6.7 us  [sum_rows(): lax.all_to_all(split, axis, split_axis=0, concat_axis=0, tiled=True)]
  transfers between devices with their start and end apart: 5 -> 2, of which waited for: 2 -> 1; matrix products, arithmetic and copies ran while one was open for 8% -> 7% of each run, Pallas kernels for 0% -> 0%
where the time goes in v1:
time: 133 us; the launch traced here: 132 us
  blocking collectives  94.2 us (71%)
  other arithmetic  11.2 us (8%)
  local copies, waits for them, and re-layouts  8.03 us (6%)
  matrix products  7.19 us (5%)
  starting transfers between devices  6.7 us (5%)
  waiting for transfers between devices  3.74 us (3%)
    all_gather x4, blocking collectives, gather_rows(): return lax.all_gather(value, axis, axis=0, tiled=True)  73.6 us
    all_to_all x2, blocking collectives, sum_rows(): lax.all_to_all(split, axis, split_axis=0, concat_axis=0, tiled=True)  20.6 us
    all_to_all x2, starting transfers between devices, sum_rows(): lax.all_to_all(split, axis, split_axis=0, concat_axis=0, tiled=True)  6.7 us
    dot_general x8, matrix products, body(): jnp.dot(normed, w[layer_id], preferred_element_type=jnp.float32)  4.85 us
    slice x1, local copies, waits for them, and re-layouts, body(): prior_state = states[layer_id]  4.72 us
    another operation x1, other arithmetic, body(): return (hidden_x, jnp.stack(outputs))  3.97 us
    add x2, other arithmetic, body(): gammas[None, :, None, None] * state_view  3.92 us
    all_to_all x2, waiting for transfers between devices, sum_rows(): lax.all_to_all(split, axis, split_axis=0, concat_axis=0, tiled=True)  3.74 us
  transfers between devices with their start and end apart: 2, of which 1 were waited for; matrix products, arithmetic and copies ran while one was open for 7% of the time, Pallas kernels for 0%

profile of v1, /device:TPU:0, one launch (start us, length us, event | category | flops | bytes accessed | tf_op | source)
XLA Modules:
  0.0 132.2 jit_solution(6076577782268910425)
XLA Ops:
  0.7 0.8 slice_convert_fusion.6
  1.5 32.5 %all_gather.12 = bf16[64,1024]{1,0:T(8,128)(2,1)S(1)} all-gather(bf16[8,1024]{1,0:T(8,128)(2,1)} %param.10), channel_id=1, replica_groups=mesh['tp'=8,'dp'=4] {'tp'}, dimensions={0}, use_global_device_ids=true | all-gather | bytes 147456 | tf_op jit(solution)/shard_map/all_gather | solution.py:41
  34.0 0.1 fusion.23
  34.5 1.3 convolution_convert_fusion.8
  35.7 1.3 convolution_convert_fusion.7
  37.0 1.3 convolution_convert_fusion.6
  38.3 0.2 convolution_convert_fusion.9
  38.5 0.8 concatenate.40
  39.2 3.3 %all-to-all-start = ((bf16[4,16,1026]{2,1,0:T(8,128)(2,1)}), bf16[4,16,1026]{2,1,0:T(8,128)(2,1)S(1)}, u32[]{:S(2)}, u32[]{:S(2)}) async-start(bf16[4,16,1026]{2,1,0:T(8,128)(2,1)} %concatenate.40), calls=%async_computation | async-start | bytes 294912 | tf_op jit(solution)/shard_map/all_to_all | solution.py:48
  42.7 4.7 %fusion.60 = (f32[1,16,256,128]{3,2,1,0:T(8,128)}, f32[1,16,256,128]{3,2,1,0:T(8,128)}) fusion(f32[2,16,256,128]{3,2,1,0:T(8,128)} %param.12), kind=kLoop, calls=%fused_computation.121 | loop fusion | bytes 8388608 | tf_op jit(solution)/shard_map/slice | solution.py:64
  47.6 0.2 fusion.57
  48.3 2.0 %multiply_add_fusion.1 = f32[16,2,128,128]{3,2,1,0:T(8,128)S(1)} fusion(f32[16,2,128,128]{3,2,1,0:T(8,128)} %bitcast.79, f32[16,2,128]{2,1,0:T(2,128)S(1)} %copy.40, f32[16,2,128]{2,1,0:T(2,128)S(1)} %reshape.248, f32[2]{0:T(128)S(1)} %exponential_subtract_fusion), kind=kLoop, calls=%fused_computation.2 | loop fusion | flops 1572864 | bytes 4227080 | tf_op jit(solution)/shard_map/add | solution.py:100
  50.3 0.6 fusion.46
  51.2 5.4 %all_gather.13 = bf16[64,256]{1,0:T(8,128)(2,1)S(1)} all-gather(bf16[16,256]{1,0:T(8,128)(2,1)S(1)} %fusion.49), channel_id=1, replica_groups=mesh['tp'=8,'dp'=4] {'dp'}, dimensions={0}, use_global_device_ids=true | all-gather | bytes 40960 | tf_op jit(solution)/shard_map/all_gather | solution.py:41
  56.6 0.2 fusion
  56.8 12.8 %all_to_all.20 = bf16[8,8,1024]{2,1,0:T(8,128)(2,1)S(1)} all-to-all(bf16[8,8,1024]{2,1,0:T(8,128)(2,1)S(1)} %fusion), channel_id=1, replica_groups=mesh['tp'=8,'dp'=4] {'tp'}, dimensions={0} | all-to-all | bytes 262144 | tf_op jit(solution)/shard_map/all_to_all | solution.py:48
  69.6 30.6 %all_gather.14 = bf16[64,1024]{1,0:T(8,128)(2,1)S(1)} all-gather(bf16[8,1024]{1,0:T(8,128)(2,1)S(1)} %add_convert_fusion.1), channel_id=1, replica_groups=mesh['tp'=8,'dp'=4] {'tp'}, dimensions={0}, use_global_device_ids=true | all-gather | bytes 147456 | tf_op jit(solution)/shard_map/all_gather | solution.py:41
  100.3 0.2 convolution_convert_fusion.4
  100.5 0.2 convolution_convert_fusion.3
  100.8 0.2 convolution_convert_fusion.2
  101.0 0.2 convolution_convert_fusion.5
  101.7 7.8 %all_to_all.21 = bf16[4,16,1026]{2,1,0:T(8,128)(2,1)S(1)} all-to-all(bf16[4,16,1026]{2,1,0:T(8,128)(2,1)S(1)} %concatenate.47), channel_id=1, replica_groups=mesh['tp'=8,'dp'=4] {'dp'}, dimensions={0} | all-to-all | bytes 262656 | tf_op jit(solution)/shard_map/all_to_all | solution.py:48
  109.5 0.2 fusion.53
  110.2 2.0 %multiply_add_fusion = f32[16,2,128,128]{3,2,1,0:T(8,128)S(1)} fusion(f32[16,2,128,128]{3,2,1,0:T(8,128)} %bitcast.78, f32[16,2,128]{2,1,0:T(2,128)S(1)} %copy.47, f32[16,2,128]{2,1,0:T(2,128)S(1)} %reshape.255, f32[2]{0:T(128)S(1)} %exponential_subtract_fusion), kind=kLoop, calls=%fused_computation.1 | loop fusion | flops 1572864 | bytes 4227080 | tf_op jit(solution)/shard_map/add | solution.py:100
  112.1 1.3 %copy-done = f32[16,2,128,128]{3,2,1,0:T(8,128)} copy-done((f32[16,2,128,128]{3,2,1,0:T(8,128)}, f32[16,2,128,128]{3,2,1,0:T(8,128)S(1)}, u32[]{:S(2)}) %copy-start) | copy-done | bytes 2097176
  113.5 0.6 fusion.44
  114.4 5.2 %all_gather.15 = bf16[64,256]{1,0:T(8,128)(2,1)S(1)} all-gather(bf16[16,256]{1,0:T(8,128)(2,1)S(1)} %fusion.48), channel_id=1, replica_groups=mesh['tp'=8,'dp'=4] {'dp'}, dimensions={0}, use_global_device_ids=true | all-gather | bytes 40960 | tf_op jit(solution)/shard_map/all_gather | solution.py:41
  119.6 0.9 fusion.1
  120.4 3.4 %all-to-all-start.3 = ((bf16[8,8,1024]{2,1,0:T(8,128)(2,1)}), bf16[8,8,1024]{2,1,0:T(8,128)(2,1)S(1)}, u32[]{:S(2)}, u32[]{:S(2)}) async-start(bf16[8,8,1024]{2,1,0:T(8,128)(2,1)} %fusion.1), calls=%async_computation.3 | async-start | bytes 262144 | tf_op jit(solution)/shard_map/all_to_all | solution.py:48
  123.8 4.0 %pad_maximum_fusion = f32[2,16,256,128]{3,2,1,0:T(8,128)} fusion(f32[1,16,256,128]{3,2,1,0:T(8,128)} %bitcast.77, f32[1,16,256,128]{3,2,1,0:T(8,128)S(1)} %bitcast.76), kind=kLoop, calls=%fused_computation | loop fusion | flops 1048576 | bytes 8388608 | tf_op jit(solution)/shard_map/stack | solution.py:119
  127.8 3.7 %all-to-all-done.3 = bf16[8,8,1024]{2,1,0:T(8,128)(2,1)S(1)} async-done(((bf16[8,8,1024]{2,1,0:T(8,128)(2,1)}), bf16[8,8,1024]{2,1,0:T(8,128)(2,1)S(1)}, u32[]{:S(2)}, u32[]{:S(2)}) %all-to-all-start.3) | async-done | bytes 131104 | tf_op jit(solution)/shard_map/all_to_all | solution.py:48
  131.6 0.6 add_convert_fusion
  (72 shorter events, 2.6 us)
Async XLA Ops:
  0.6 37.6 %copy-start.7 = (bf16[2,1024,256]{2,1,0:T(8,128)(2,1)S(1)}, bf16[2,1024,256]{2,1,0:T(8,128)(2,1)}, u32[]{:S(2)}) copy-start(bf16[2,1024,256]{2,1,0:T(8,128)(2,1)} %param.14) | copy-start | bytes 3145732
  0.6 42.0 %copy-start.9 = (s32[16]{0:T(128)S(1)}, s32[16]{0:T(128)}, u32[]{:S(2)}) copy-start(s32[16]{0:T(128)} %param.11) | copy-start | bytes 196
  0.7 42.0 %copy-start.3 = (bf16[2,256]{1,0:T(2,128)(2,1)S(1)}, bf16[2,256]{1,0:T(2,128)(2,1)}, u32[]{:S(2)}) copy-start(bf16[2,256]{1,0:T(2,128)(2,1)} %param.18) | copy-start | bytes 3076
  39.2 8.3 %all-to-all-start = ((bf16[4,16,1026]{2,1,0:T(8,128)(2,1)}), bf16[4,16,1026]{2,1,0:T(8,128)(2,1)S(1)}, u32[]{:S(2)}, u32[]{:S(2)}) async-start(bf16[4,16,1026]{2,1,0:T(8,128)(2,1)} %concatenate.40), calls=%async_computation | async-start | bytes 294912 | tf_op jit(solution)/shard_map/all_to_all | solution.py:48
  50.2 6.3 %copy-start.1 = (bf16[2,256,1024]{2,1,0:T(8,128)(2,1)S(1)}, bf16[2,256,1024]{2,1,0:T(8,128)(2,1)}, u32[]{:S(2)}) copy-start(bf16[2,256,1024]{2,1,0:T(8,128)(2,1)} %param.19) | copy-start | bytes 3145732
  50.2 19.3 %copy-start.2 = (bf16[8,1024]{1,0:T(8,128)(2,1)S(1)}, bf16[8,1024]{1,0:T(8,128)(2,1)}, u32[]{:S(2)}) copy-start(bf16[8,1024]{1,0:T(8,128)(2,1)} %param.10) | copy-start | bytes 49156
  50.3 50.0 %copy-start.4 = (bf16[2,1024,256]{2,1,0:T(8,128)(2,1)S(1)}, bf16[2,1024,256]{2,1,0:T(8,128)(2,1)}, u32[]{:S(2)}) copy-start(bf16[2,1024,256]{2,1,0:T(8,128)(2,1)} %param.15) | copy-start | bytes 3145732
  50.3 50.3 %copy-start.5 = (bf16[2,1024,256]{2,1,0:T(8,128)(2,1)S(1)}, bf16[2,1024,256]{2,1,0:T(8,128)(2,1)}, u32[]{:S(2)}) copy-start(bf16[2,1024,256]{2,1,0:T(8,128)(2,1)} %param.16) | copy-start | bytes 3145732
  50.9 49.8 %copy-start.6 = (bf16[2,1024,256]{2,1,0:T(8,128)(2,1)S(1)}, bf16[2,1024,256]{2,1,0:T(8,128)(2,1)}, u32[]{:S(2)}) copy-start(bf16[2,1024,256]{2,1,0:T(8,128)(2,1)} %param.17) | copy-start | bytes 3145732
  50.9 50.1 %copy-start.8 = (bf16[2,1024,256]{2,1,0:T(8,128)(2,1)S(1)}, bf16[2,1024,256]{2,1,0:T(8,128)(2,1)}, u32[]{:S(2)}) copy-start(bf16[2,1024,256]{2,1,0:T(8,128)(2,1)} %param.14) | copy-start | bytes 3145732
  112.1 1.4 %copy-start = (f32[16,2,128,128]{3,2,1,0:T(8,128)}, f32[16,2,128,128]{3,2,1,0:T(8,128)S(1)}, u32[]{:S(2)}) copy-start(f32[16,2,128,128]{3,2,1,0:T(8,128)S(1)} %multiply_add_fusion) | copy-start | bytes 6291460
  120.4 11.1 %all-to-all-start.3 = ((bf16[8,8,1024]{2,1,0:T(8,128)(2,1)}), bf16[8,8,1024]{2,1,0:T(8,128)(2,1)S(1)}, u32[]{:S(2)}, u32[]{:S(2)}) async-start(bf16[8,8,1024]{2,1,0:T(8,128)(2,1)} %fusion.1), calls=%async_computation.3 | async-start | bytes 262144 | tf_op jit(solution)/shard_map/all_to_all | solution.py:48
